TPU v7x, 32 devices: a whole 2x2x4 slice. The times are simulated.
32 devices in a mesh: grp: 2 (over y), tp: 4 (over z), dp: 4 (over x, core).
Axes of the slice: x: 2, y: 2, z: 4, core: 2. Of those that a mesh axis runs over, the one named last changes fastest.
Arguments:
- tokens: bfloat16 [128, 2048], P(('grp', 'tp'), 'dp'), parts along dimension 0, may hold values from -200 to 200
- norm_gain: bfloat16 [2, 2048], P(None, 'dp'), may hold values from 0.099609375 to 1.8984375
- w_z: bfloat16 [2, 2048, 4096], P(None, 'dp', 'tp'), may hold values from -0.125 to 0.125
- w_x: bfloat16 [2, 2048, 4096], P(None, 'dp', 'tp'), may hold values from -0.125 to 0.125
- w_b: bfloat16 [2, 2048, 1024], P(None, 'dp', 'tp'), may hold values from -0.125 to 0.125
- w_c: bfloat16 [2, 2048, 1024], P(None, 'dp', 'tp'), may hold values from -0.125 to 0.125
- w_dt: bfloat16 [2, 2048, 64], P(None, 'dp'), may hold values from -0.125 to 0.125
- conv_x: bfloat16 [2, 4, 4096], P(None, None, 'tp'), may hold values from -3 to 3
- conv_b: bfloat16 [2, 4, 1024], P(None, None, 'tp'), may hold values from -3 to 3
- conv_c: bfloat16 [2, 4, 1024], P(None, None, 'tp'), may hold values from -3 to 3
- dt_bias: float32 [2, 64], P(None, 'tp'), may hold values from -3 to 0.5
- a_log: float32 [2, 64], P(None, 'tp'), may hold values from 0 to 2.5
- d_skip: float32 [2, 64], P(None, 'tp'), may hold values from 0.5 to 2
- out_gain: bfloat16 [2, 4096], P(None, 'tp'), may hold values from 0.099609375 to 1.8984375
- w_out: bfloat16 [2, 4096, 2048], P(None, 'tp', 'dp'), may hold values from -0.09375 to 0.09375
- ssm_state: float32 [2, 128, 64, 64, 64], P(None, ('grp', 'dp'), 'tp'), parts along dimension 1, may hold values from -3 to 3
- state_x: bfloat16 [2, 128, 3, 4096], P(None, ('grp', 'dp'), None, 'tp'), parts along dimension 1, may hold values from -6 to 6
- state_b: bfloat16 [2, 128, 3, 1024], P(None, ('grp', 'dp'), None, 'tp'), parts along dimension 1, may hold values from -6 to 6
- state_c: bfloat16 [2, 128, 3, 1024], P(None, ('grp', 'dp'), None, 'tp'), parts along dimension 1, may hold values from -6 to 6
Outputs:
- residual: bfloat16 [128, 2048], P(('grp', 'tp'), 'dp'), parts along dimension 0
- ssm_next: float32 [2, 128, 64, 64, 64], P(None, ('grp', 'dp'), 'tp'), parts along dimension 1
- next_x: bfloat16 [2, 128, 3, 4096], P(None, ('grp', 'dp'), None, 'tp'), parts along dimension 1
- next_b: bfloat16 [2, 128, 3, 1024], P(None, ('grp', 'dp'), None, 'tp'), parts along dimension 1
- next_c: bfloat16 [2, 128, 3, 1024], P(None, ('grp', 'dp'), None, 'tp'), parts along dimension 1
There are 2 independent parts, one for each index of `grp`. A program takes and returns all parts, laid end to end along the dimension named above; an argument that names none is the same for every part. Nothing has to cross between parts.
All inputs are finite; a program needn't handle non-finite values.
Results may differ from a plain program's by a relative error of at most 0.0095.
Values may be sent and summed in bfloat16 or wider, within the bound.
A program may use at most 128 MiB of HBM per device.

v0:
```python
import jax
import jax.numpy as jnp
from jax import lax
from jax.sharding import PartitionSpec as P

HEAD_DIM = 64
STATE = 64


EPSILON = 1e-05


def convolve(history, latest, weight):
    window = jnp.concatenate([history, latest[:, None, :]], axis=1)
    summed = jnp.sum(window.astype(jnp.float32) * weight.astype(jnp.float32)[None], axis=1)
    return (jax.nn.silu(summed), window[:, 1:])


def mixer(gate_in, conv_xv, conv_bv, conv_cv, step_raw, bias, log_rate, skip, gain, state_prev):
    seq_count = conv_xv.shape[0]
    heads_here = step_raw.shape[1]
    group_count = conv_bv.shape[1] // STATE
    per_group = heads_here // group_count
    step_size = jax.nn.softplus(step_raw + bias)
    decay_rate = jnp.exp(-step_size * jnp.exp(log_rate))
    x_heads = conv_xv.reshape(seq_count, group_count, per_group, HEAD_DIM)
    b_state = conv_bv.reshape(seq_count, group_count, 1, 1, STATE)
    c_state = conv_cv.reshape(seq_count, group_count, 1, 1, STATE)
    step_heads = step_size.reshape(seq_count, group_count, per_group, 1)
    decay_heads = decay_rate.reshape(seq_count, group_count, per_group, 1, 1)
    previous = state_prev.reshape(seq_count, group_count, per_group, HEAD_DIM, STATE)
    state_next = decay_heads * previous + (step_heads * x_heads)[..., None] * b_state
    readout = (
        jnp.sum(state_next * c_state, axis=-1)
        + skip.reshape(1, group_count, per_group, 1) * x_heads
    )
    gated_out = readout.reshape(seq_count, group_count, -1) * jax.nn.silu(
        gate_in.astype(jnp.float32)
    ).reshape(seq_count, group_count, -1)
    normed = gated_out * lax.rsqrt(
        jnp.mean(gated_out * gated_out, axis=-1, keepdims=True) + EPSILON
    )
    mixed_out = (normed.reshape(seq_count, -1) * gain.astype(jnp.float32)).astype(jnp.bfloat16)
    return (mixed_out, state_next.reshape(seq_count, heads_here, HEAD_DIM, STATE))


def body(
    tokens,
    norm_gain,
    w_z,
    w_x,
    w_b,
    w_c,
    w_dt,
    conv_x,
    conv_b,
    conv_c,
    dt_bias,
    a_log,
    d_skip,
    out_gain,
    w_out,
    ssm_state,
    state_x,
    state_b,
    state_c,
):
    dp_size = lax.axis_size("dp")
    residual = tokens
    states, saved_x, saved_b, saved_c = ([], [], [], [])
    width_z = w_z.shape[2]
    width_b = w_b.shape[2]
    width_dt = w_dt.shape[2]
    for layer_index in range(w_z.shape[0]):
        gathered_rows = lax.all_gather(residual, "tp", axis=0, tiled=True)
        seq_dev = gathered_rows.shape[0] // dp_size
        features = gathered_rows.shape[1] * dp_size
        widened = gathered_rows.astype(jnp.float32)
        squares = jnp.sum(widened * widened, axis=1)
        scaled = (widened * norm_gain[layer_index].astype(jnp.float32)).astype(jnp.bfloat16)
        matrices = (
            w_z[layer_index],
            w_x[layer_index],
            w_b[layer_index],
            w_c[layer_index],
            w_dt[layer_index],
        )
        pieces = 1
        piece_rows = seq_dev // pieces
        rows_piece = scaled.reshape(dp_size, seq_dev, -1).reshape(dp_size * piece_rows, -1)
        columns = [
            jnp.dot(rows_piece, matrix, preferred_element_type=jnp.float32) for matrix in matrices
        ]
        merged_terms = jnp.concatenate(columns, axis=1)
        collected = lax.psum_scatter(merged_terms, "dp", scatter_dimension=0, tiled=True)
        everything = lax.psum(squares, "dp")
        total_squares = lax.dynamic_slice_in_dim(
            everything, lax.axis_index("dp") * seq_dev, seq_dev, 0
        )
        row_scale = lax.rsqrt(total_squares / features + EPSILON)[:, None]
        gate_in = (collected[:, 0:width_z] * row_scale).astype(jnp.bfloat16)
        x_in = (collected[:, width_z : 2 * width_z] * row_scale).astype(jnp.bfloat16)
        b_in = (collected[:, 2 * width_z : 2 * width_z + width_b] * row_scale).astype(jnp.bfloat16)
        c_in = (collected[:, 2 * width_z + width_b : 2 * width_z + 2 * width_b] * row_scale).astype(
            jnp.bfloat16
        )
        step_all = (
            collected[:, 2 * width_z + 2 * width_b : 2 * width_z + 2 * width_b + width_dt]
            * row_scale
        )
        heads_here = dt_bias.shape[1]
        step_raw = lax.dynamic_slice_in_dim(
            step_all, lax.axis_index("tp") * heads_here, heads_here, 1
        )
        conv_xv, kept_x = convolve(state_x[layer_index], x_in, conv_x[layer_index])
        conv_bv, kept_b = convolve(state_b[layer_index], b_in, conv_b[layer_index])
        conv_cv, kept_c = convolve(state_c[layer_index], c_in, conv_c[layer_index])
        mixed_out, state_next = mixer(
            gate_in,
            conv_xv,
            conv_bv,
            conv_cv,
            step_raw,
            dt_bias[layer_index],
            a_log[layer_index],
            d_skip[layer_index],
            out_gain[layer_index],
            ssm_state[layer_index],
        )
        all_mixed = lax.all_gather(mixed_out, "dp", axis=0, tiled=True)
        weight_out = w_out[layer_index]

        def head_term(first_row, row_count, source=all_mixed, matrix=weight_out):
            return jnp.dot(source, matrix, preferred_element_type=jnp.float32)

        projected = lax.psum_scatter(
            head_term(jnp.int32(0), lax.axis_size("tp") * residual.shape[0]),
            "tp",
            scatter_dimension=0,
            tiled=True,
        )
        residual = (residual.astype(jnp.float32) + projected).astype(jnp.bfloat16)
        states.append(state_next)
        saved_x.append(kept_x)
        saved_b.append(kept_b)
        saved_c.append(kept_c)
    return (residual, jnp.stack(states), jnp.stack(saved_x), jnp.stack(saved_b), jnp.stack(saved_c))


def solution(mesh):
    placed = (
        P(("grp", "tp"), "dp"),
        P(None, "dp"),
        P(None, "dp", "tp"),
        P(None, "dp", "tp"),
        P(None, "dp", "tp"),
        P(None, "dp", "tp"),
        P(None, "dp", None),
        P(None, None, "tp"),
        P(None, None, "tp"),
        P(None, None, "tp"),
        P(None, "tp"),
        P(None, "tp"),
        P(None, "tp"),
        P(None, "tp"),
        P(None, "tp", "dp"),
        P(None, ("grp", "dp"), "tp", None, None),
        P(None, ("grp", "dp"), None, "tp"),
        P(None, ("grp", "dp"), None, "tp"),
        P(None, ("grp", "dp"), None, "tp"),
    )
    return jax.shard_map(
        body,
        mesh=mesh,
        in_specs=placed,
        out_specs=(
            P(("grp", "tp"), "dp"),
            P(None, ("grp", "dp"), "tp", None, None),
            P(None, ("grp", "dp"), None, "tp"),
            P(None, ("grp", "dp"), None, "tp"),
            P(None, ("grp", "dp"), None, "tp"),
        ),
        check_vma=False,
    )
```

profile of v0, /device:TPU:0, one launch (start us, length us, event | category | flops | bytes accessed | tf_op | source)
XLA Modules:
  0.0 179.7 jit_solution(405704557160947829)
XLA Ops:
  7.2 15.1 %all_gather.12 = bf16[64,512]{1,0:T(8,128)(2,1)S(1)} all-gather(bf16[16,512]{1,0:T(8,128)(2,1)} %param.19), channel_id=1, replica_groups=mesh['grp'=2,'tp'=4,'dp'=4] {'tp'}, dimensions={0}, use_global_device_ids=true | all-gather | bytes 81920 | tf_op jit(solution)/shard_map/all_gather | solution.py:75
  23.1 1.5 convolution_dynamic-update-slice_fusion.3
  24.6 1.5 convolution_dynamic-update-slice_fusion.2
  26.2 1.1 convolution_dynamic-update-slice_fusion.7
  27.3 1.1 convolution_dynamic-update-slice_fusion.6
  28.4 1.0 convolution_dynamic-update-slice_fusion.9
  29.4 0.8 copy-done.1
  31.5 5.6 %psum.14 = f32[64]{0:T(128)S(1)} all-reduce(f32[64]{0:T(128)S(1)} %fusion.23), channel_id=1, replica_groups=mesh['grp'=2,'tp'=4,'dp'=4] {'dp'}, use_global_device_ids=true, to_apply=%region_2.0 | all-reduce | flops 64 | bytes 512 | tf_op jit(solution)/shard_map/psum | solution.py:96
  42.5 1.0 slice_bitcast_fusion
  43.4 10.8 %reduce-scatter.5.cloned.1.call-done = f32[16,2624]{1,0:T(8,128)} async-done(((f32[64,2624]{1,0:T(8,128)}), f32[16,2624]{1,0:T(8,128)}) %reduce-scatter.5.cloned.1.call-update) | async-done | bytes 167952 | tf_op jit(solution)/shard_map/reduce_scatter | solution.py:95
  54.2 1.0 fusion.44
  55.3 0.8 fusion.68
  57.4 8.5 %multiply_reduce_fusion.1 = (f32[16,16,64]{2,1,0:T(8,128)S(1)}, f32[1,16,16,64,64]{4,3,2,1,0:T(8,128)}) fusion(f32[16,16,64]{2,1,0:T(8,128)S(1)} %bitcast.112, f32[16,16,64]{2,1,0:T(8,128)S(1)} %bitcast.114, f32[16,16,64]{2,1,0:T(8,128)S(1)} %multiply_multiply_fusion.1, f32[2,16,16,64,64]{4,3,2,1,0:T(8,128)} %param.34, f32[16,16]{1,0:T(8,128)S(1)} %get-tuple-element.13), kind=kLoop, calls=%fused_computation.3 | loop fusion | flops 5226496 | bytes 8651776 | tf_op jit(solution)/shard_map/reduce_sum | solution.py:34
  66.5 5.4 %all_gather.13 = bf16[64,1024]{1,0:T(8,128)(2,1)S(1)} all-gather(bf16[16,1024]{1,0:T(8,128)(2,1)S(1)} %multiply_convert_fusion.1), channel_id=1, replica_groups=mesh['grp'=2,'tp'=4,'dp'=4] {'dp'}, dimensions={0}, use_global_device_ids=true | all-gather | bytes 163840 | tf_op jit(solution)/shard_map/all_gather | solution.py:130
  71.9 1.0 fusion.4
  72.9 19.5 %reduce-scatter.7.cloned.1.call-done = f32[16,512]{1,0:T(8,128)} async-done(((f32[64,512]{1,0:T(8,128)}), f32[16,512]{1,0:T(8,128)}) %reduce-scatter.7.cloned.1.call-update) | async-done | bytes 32784 | tf_op jit(solution)/shard_map/reduce_scatter | solution.py:136
  93.2 13.1 %all_gather.14 = bf16[64,512]{1,0:T(8,128)(2,1)S(1)} all-gather(bf16[16,512]{1,0:T(8,128)(2,1)S(1)} %add_convert_fusion.1), channel_id=1, replica_groups=mesh['grp'=2,'tp'=4,'dp'=4] {'tp'}, dimensions={0}, use_global_device_ids=true | all-gather | bytes 81920 | tf_op jit(solution)/shard_map/all_gather | solution.py:75
  106.3 1.5 convolution_dynamic-update-slice_fusion.1
  107.9 1.5 convolution_dynamic-update-slice_fusion
  109.4 1.1 convolution_dynamic-update-slice_fusion.5
  110.5 1.1 convolution_dynamic-update-slice_fusion.4
  111.8 0.8 copy-done.2
  113.2 5.7 %psum.15 = f32[64]{0:T(128)S(1)} all-reduce(f32[64]{0:T(128)S(1)} %fusion.25), channel_id=1, replica_groups=mesh['grp'=2,'tp'=4,'dp'=4] {'dp'}, use_global_device_ids=true, to_apply=%region_11.12 | all-reduce | flops 64 | bytes 512 | tf_op jit(solution)/shard_map/psum | solution.py:96
  118.9 14.7 %reduce-scatter.9.cloned.1.call-done = f32[16,2624]{1,0:T(8,128)} async-done(((f32[64,2624]{1,0:T(8,128)}), f32[16,2624]{1,0:T(8,128)}) %reduce-scatter.9.cloned.1.call-update) | async-done | bytes 167952 | tf_op jit(solution)/shard_map/reduce_scatter | solution.py:95
  133.6 1.0 fusion.45
  134.8 0.8 fusion.70
  136.8 8.4 %multiply_reduce_fusion = (f32[16,16,64]{2,1,0:T(8,128)S(1)}, f32[1,16,16,64,64]{4,3,2,1,0:T(8,128)}) fusion(f32[16,16,64]{2,1,0:T(8,128)S(1)} %bitcast.113, f32[16,16,64]{2,1,0:T(8,128)S(1)} %bitcast.115, f32[16,16,64]{2,1,0:T(8,128)S(1)} %multiply_multiply_fusion, f32[2,16,16,64,64]{4,3,2,1,0:T(8,128)} %param.34, f32[16,16]{1,0:T(8,128)S(1)} %get-tuple-element.9), kind=kLoop, calls=%fused_computation.1 | loop fusion | flops 5226496 | bytes 8651776 | tf_op jit(solution)/shard_map/reduce_sum | solution.py:34
  145.8 5.4 %all_gather.15 = bf16[64,1024]{1,0:T(8,128)(2,1)S(1)} all-gather(bf16[16,1024]{1,0:T(8,128)(2,1)S(1)} %multiply_convert_fusion), channel_id=1, replica_groups=mesh['grp'=2,'tp'=4,'dp'=4] {'dp'}, dimensions={0}, use_global_device_ids=true | all-gather | bytes 163840 | tf_op jit(solution)/shard_map/all_gather | solution.py:130
  151.2 0.9 fusion
  152.1 12.5 %pad_maximum_fusion = f32[2,16,16,64,64]{4,3,2,1,0:T(8,128)} fusion(f32[1,16,16,64,64]{4,3,2,1,0:T(8,128)} %get-tuple-element.8, f32[1,16,16,64,64]{4,3,2,1,0:T(8,128)} %get-tuple-element.12), kind=kLoop, calls=%fused_computation | loop fusion | flops 2097152 | bytes 16777216 | tf_op jit(solution)/shard_map/stack | solution.py:147
  166.6 5.2 %reduce-scatter.11.cloned.1.call-done = f32[16,512]{1,0:T(8,128)} async-done(((f32[64,512]{1,0:T(8,128)}), f32[16,512]{1,0:T(8,128)}) %reduce-scatter.11.cloned.1.call-update) | async-done | bytes 32784 | tf_op jit(solution)/shard_map/reduce_scatter | solution.py:136
  171.8 1.4 add_convert_fusion
  (90 shorter events, 14.6 us)
Async XLA Ops:
  7.2 47.0 %reduce-scatter.5.cloned.1.call-start = ((), (), s32[]{:S(2)}) async-start(), calls=%async_computation.4 | async-start | bytes 860160 | tf_op jit(solution)/shard_map/reduce_scatter | solution.py:95
  29.4 0.8 copy-start.1
  30.3 62.2 %reduce-scatter.7.cloned.1.call-start = ((), (), s32[]{:S(2)}) async-start(), calls=%async_computation.5 | async-start | bytes 163840 | tf_op jit(solution)/shard_map/reduce_scatter | solution.py:136
  57.4 14.5 %copy-start = (bf16[2,1024,512]{2,1,0:T(8,128)(2,1)S(1)}, bf16[2,1024,512]{2,1,0:T(8,128)(2,1)}, u32[]{:S(2)}) copy-start(bf16[2,1024,512]{2,1,0:T(8,128)(2,1)} %param.33) | copy-start | bytes 6291460
  57.4 35.1 %copy-start.3 = (bf16[16,512]{1,0:T(8,128)(2,1)S(1)}, bf16[16,512]{1,0:T(8,128)(2,1)}, u32[]{:S(2)}) copy-start(bf16[16,512]{1,0:T(8,128)(2,1)} %param.19) | copy-start | bytes 49156
  57.4 54.3 %copy-start.4 = (bf16[2,512,64]{1,2,0:T(8,128)(2,1)S(1)}, bf16[2,512,64]{1,2,0:T(8,128)(2,1)}, u32[]{:S(2)}) copy-start(bf16[2,512,64]{1,2,0:T(8,128)(2,1)} %param.25) | copy-start | bytes 393220
  72.9 60.8 %reduce-scatter.9.cloned.1.call-start = ((), (), s32[]{:S(2)}) async-start(), calls=%async_computation.6 | async-start | bytes 860160 | tf_op jit(solution)/shard_map/reduce_scatter | solution.py:95
  111.8 0.9 copy-start.2
  112.7 59.1 %reduce-scatter.11.cloned.1.call-start = ((), (), s32[]{:S(2)}) async-start(), calls=%async_computation.7 | async-start | bytes 163840 | tf_op jit(solution)/shard_map/reduce_scatter | solution.py:136
Sparse Core Ops, SparseCore 0:
  30.4 23.7 reduce-scatter.4
  73.0 19.4 reduce-scatter.6
  112.8 20.7 reduce-scatter.8
  152.3 19.4 reduce-scatter.10
where the time goes:
time: 181 us; the launch traced here: 180 us
  blocking collectives  50.4 us (28%)
  waiting for transfers between devices  50.2 us (28%)
  other arithmetic  42.1 us (23%)
  between operations  14.1 us (8%)
  matrix products  13.6 us (8%)
  local copies, waits for them, and re-layouts  9.09 us (5%)
    all_gather x2, blocking collectives, body(): gathered_rows = lax.all_gather(residual, 'tp', axis=0, tiled=True)  28.3 us
    reduce_scatter x2, waiting for transfers between devices, body(): lax.psum_scatter(merged_terms, 'dp', scatter_dimension=0, tiled=True)  25.5 us
    reduce_scatter x2, waiting for transfers between devices, body(): lax.psum_scatter(head_term(jnp.int32(0), lax.axis_size('tp') * residual.s...  24.7 us
    reduce_sum x2, other arithmetic, mixer(): jnp.sum(state_next * c_state, axis=-1)  16.9 us
    another operation x1, other arithmetic, body(): jnp.stack(states)  12.5 us
    dot_general x10, matrix products, body(): jnp.dot(rows_piece, matrix, preferred_element_type=jnp.float32)  11.7 us
    psum x2, blocking collectives, body(): everything = lax.psum(squares, 'dp')  11.3 us
    all_gather x2, blocking collectives, body(): all_mixed = lax.all_gather(mixed_out, 'dp', axis=0, tiled=True)  10.8 us
  transfers between devices with their start and end apart: 4, of which 4 were waited for; matrix products, arithmetic and copies ran while one was open for 12% of the time, Pallas kernels for 0%

commit v1 on v0

v1 whole, which is shorter than its diff:
```python
import functools

import jax
import jax.numpy as jnp
from jax import lax
from jax.experimental import pallas as pl
from jax.experimental.pallas import tpu as pltpu
from jax.sharding import PartitionSpec as P

HEAD_DIM = 64
STATE = 64
LANES = 128
EPSILON = 1e-05
MESH = pl.DeviceIdType.MESH
HBM = pl.BlockSpec(memory_space=pl.ANY)
VMEM = pl.BlockSpec(memory_space=pltpu.VMEM)


def padded(width):
    return -(-width // LANES) * LANES


def enter(sizes):
    barrier = pltpu.get_barrier_semaphore()
    count = 0
    for axis, size in sizes:
        me = lax.axis_index(axis)
        for k in range(1, size):
            pl.semaphore_signal(
                barrier, inc=1, device_id={axis: lax.rem(me + k, size)}, device_id_type=MESH
            )
            count += 1
    pl.semaphore_wait(barrier, count)


def push(axis, size, k, source, target, sems):
    me = lax.axis_index(axis)
    send, recv = sems
    return pltpu.make_async_remote_copy(
        src_ref=source,
        dst_ref=target,
        send_sem=send,
        recv_sem=recv,
        device_id={axis: lax.rem(me + k, size)},
        device_id_type=MESH,
    )


def start_loads(layer, pairs, sems):
    loads = []
    for i, (source, target) in enumerate(pairs):
        load = pltpu.make_async_copy(source.at[layer], target, sems.at[i])
        load.start()
        loads.append(load)
    return loads


def front(dims, layer, rows_ref, gain_ref, loads, scratch, outs):
    tp, dp, features = dims
    (wz, wx, wb, wc, wdt, gathered, total, half, got, side, side_got, sems) = scratch
    (ag_s, ag_r, rs_s, rs_r) = sems
    act_ref, step_ref = outs
    me_tp, me_dp = lax.axis_index("tp"), lax.axis_index("dp")
    rows, block = rows_ref.shape
    seqs = tp * rows // dp
    copies = []
    for k in range(1, tp):
        copy = push("tp", tp, k, rows_ref, gathered.at[me_tp], (ag_s.at[k], ag_r.at[k]))
        copy.start()
        copies.append(copy)
    gathered[me_tp] = rows_ref[...]
    for copy in copies:
        copy.wait()
    widened = gathered[...].reshape(tp * rows, block).astype(jnp.float32)
    scaled = (widened * gain_ref[layer : layer + 1, :].astype(jnp.float32)).astype(jnp.bfloat16)
    squares = jnp.sum(widened * widened, axis=1, keepdims=True)
    width, state_width, dt_width = wx.shape[1], wb.shape[1], wdt.shape[0]
    state_pad = padded(state_width)

    for load in loads:
        load.wait()
    dt = lax.dot_general(
        scaled, wdt[...], (((1,), (1,)), ((), ())), preferred_element_type=jnp.float32
    )
    side[...] = jnp.broadcast_to(squares, (dp * seqs, side.shape[2])).reshape(side.shape)
    side[:, :, 0:dt_width] = dt.reshape(dp, seqs, dt_width)
    copies = []
    for k in range(1, dp):
        peer = lax.rem(me_dp + k, dp)
        copy = push(
            "dp", dp, k, side.at[peer], side_got.at[k - 1], (rs_s.at[0, k], rs_r.at[0, k])
        )
        copy.start()
        copies.append(copy)
    spans = ((0, 0, wz, width), (1, 0, wx, width), (1, width, wb, state_width))
    spans = spans + ((1, width + state_pad, wc, state_width),)
    offsets = (0, width)
    for index, (piece, at, weight, size) in enumerate(spans):
        term = jnp.dot(scaled, weight[...], preferred_element_type=jnp.float32)
        term = term.reshape(dp, seqs, size)
        base = offsets[piece] + at
        total[:, :, base : base + size] = term
        half[piece][:, :, at : at + size] = term.astype(jnp.bfloat16)
        if index in (0, len(spans) - 1):
            for k in range(1, dp):
                peer = lax.rem(me_dp + k, dp)
                copy = push(
                    "dp",
                    dp,
                    k,
                    half[piece].at[peer],
                    got[piece].at[k - 1],
                    (rs_s.at[1 + piece, k], rs_r.at[1 + piece, k]),
                )
                copy.start()
                copies.append(copy)
    for copy in copies[: dp - 1]:
        copy.wait()
    side_sum = side[me_dp]
    for k in range(1, dp):
        side_sum = side_sum + side_got[k - 1]
    row_scale = lax.rsqrt(side_sum[:, LANES : LANES + 1] / features + EPSILON)
    step_ref[...] = side_sum[:, 0:LANES] * row_scale
    edges = (0, width, total.shape[2])
    for piece in range(2):
        for copy in copies[(piece + 1) * (dp - 1) : (piece + 2) * (dp - 1)]:
            copy.wait()
        value = total[me_dp, :, edges[piece] : edges[piece + 1]]
        for k in range(1, dp):
            value = value + got[piece][k - 1].astype(jnp.float32)
        act_ref[:, edges[piece] : edges[piece + 1]] = (value * row_scale).astype(jnp.bfloat16)


def back(dims, mixed_ref, rows_ref, load, scratch, out_ref):
    tp, dp, _ = dims
    wo, gathered, total, half, got, sems = scratch
    ag_s, ag_r, rs_s, rs_r = sems
    me_tp, me_dp = lax.axis_index("tp"), lax.axis_index("dp")
    seqs, width = mixed_ref.shape
    rows, block = rows_ref.shape
    copies = []
    for k in range(1, dp):
        copy = push("dp", dp, k, mixed_ref, gathered.at[me_dp], (ag_s.at[k], ag_r.at[k]))
        copy.start()
        copies.append(copy)
    gathered[me_dp] = mixed_ref[...]
    for copy in copies:
        copy.wait()
    load.wait()
    term = jnp.dot(
        gathered[...].reshape(dp * seqs, width), wo[...], preferred_element_type=jnp.float32
    ).reshape(tp, rows, block)
    total[...] = term
    half[...] = term.astype(jnp.bfloat16)
    copies = []
    for k in range(1, tp):
        peer = lax.rem(me_tp + k, tp)
        copy = push("tp", tp, k, half.at[peer], got.at[k - 1], (rs_s.at[k], rs_r.at[k]))
        copy.start()
        copies.append(copy)
    value = total[me_tp]
    for copy in copies:
        copy.wait()
    for k in range(1, tp):
        value = value + got[k - 1].astype(jnp.float32)
    out_ref[...] = (rows_ref[...].astype(jnp.float32) + value).astype(jnp.bfloat16)


def front_scratch(dims, rows, block, w_x, w_b, dt_width):
    tp, dp, _ = dims
    seqs = tp * rows // dp
    width, state = w_x.shape[2], w_b.shape[2]
    both = width + 2 * padded(state)
    bf, f32, dma = jnp.bfloat16, jnp.float32, pltpu.SemaphoreType.DMA
    weights = [
        pltpu.VMEM((block, width), bf),
        pltpu.VMEM((block, width), bf),
        pltpu.VMEM((block, state), bf),
        pltpu.VMEM((block, state), bf),
        pltpu.VMEM((dt_width, block), bf),
    ]
    rest = [
        pltpu.VMEM((tp, rows, block), bf),
        pltpu.VMEM((dp, seqs, width + both), f32),
        pltpu.VMEM((dp, seqs, width), bf),
        pltpu.VMEM((dp, seqs, both), bf),
        pltpu.VMEM((dp - 1, seqs, width), bf),
        pltpu.VMEM((dp - 1, seqs, both), bf),
        pltpu.VMEM((dp, seqs, 2 * LANES), f32),
        pltpu.VMEM((dp - 1, seqs, 2 * LANES), f32),
        dma((tp,)),
        dma((tp,)),
        dma((3, dp)),
        dma((3, dp)),
        dma((5,)),
    ]
    return weights + rest


def back_scratch(dims, rows, block, width):
    tp, dp, _ = dims
    seqs = tp * rows // dp
    bf, f32, dma = jnp.bfloat16, jnp.float32, pltpu.SemaphoreType.DMA
    return [
        pltpu.VMEM((width, block), bf),
        pltpu.VMEM((dp, seqs, width), bf),
        pltpu.VMEM((tp, rows, block), f32),
        pltpu.VMEM((tp, rows, block), bf),
        pltpu.VMEM((tp - 1, rows, block), bf),
        dma((dp,)),
        dma((dp,)),
        dma((tp,)),
        dma((tp,)),
        dma((1,)),
    ]


FRONT = 18
BACK = 10


def split_front(refs):
    wz, wx, wb, wc, wdt, gathered, total, h0, h1, g0, g1, side, side_got = refs[:13]
    scratch = (wz, wx, wb, wc, wdt, gathered, total, (h0, h1), (g0, g1), side, side_got)
    return scratch + (refs[13:17],), refs[17]


def kernel(dims, layer, has_back, has_front, *refs):
    tp, dp, _ = dims
    refs = list(refs)
    take = lambda n: [refs.pop(0) for _ in range(n)]
    rows_ref = take(1)[0]
    if has_back:
        mixed_ref, wo_ref = take(2)
    if has_front:
        gain_ref, *weights = take(6)
    new_ref = take(1)[0] if has_back else rows_ref
    outs = take(2) if has_front else None
    back_refs = take(BACK) if has_back else None
    front_refs = take(FRONT) if has_front else None
    if has_back:
        load = pltpu.make_async_copy(wo_ref.at[layer], back_refs[0], back_refs[-1].at[0])
        load.start()
    if has_front:
        scratch, load_sems = split_front(front_refs)
        here = layer + 1 if has_back else layer
        loads = start_loads(here, list(zip(weights, scratch[:5])), load_sems)
    enter((("tp", tp), ("dp", dp)))
    if has_back:
        pieces = tuple(back_refs[:5]) + (back_refs[5:9],)
        back(dims, mixed_ref, rows_ref, load, pieces, new_ref)
    if has_front:
        front(dims, here, new_ref, gain_ref, loads, scratch, outs)


def exchange(dims, number, layer, rows, mixed, w_out, norm_gain, weights):
    has_back, has_front = mixed is not None, weights is not None
    tp, dp, _ = dims
    count, block = rows.shape
    seqs = tp * count // dp
    operands, specs, shapes, scratch = [rows], [VMEM], [], []
    if has_back:
        operands += [mixed, w_out]
        specs += [VMEM, HBM]
        shapes.append(jax.ShapeDtypeStruct(rows.shape, jnp.bfloat16))
        scratch += back_scratch(dims, count, block, mixed.shape[1])
    if has_front:
        operands += [norm_gain, *weights]
        specs += [VMEM] + [HBM] * 5
        w_x, w_b, w_dt = weights[1], weights[2], weights[4]
        across = 2 * w_x.shape[2] + 2 * padded(w_b.shape[2])
        shapes.append(jax.ShapeDtypeStruct((seqs, across), jnp.bfloat16))
        shapes.append(jax.ShapeDtypeStruct((seqs, LANES), jnp.float32))
        scratch += front_scratch(dims, count, block, w_x, w_b, w_dt.shape[1])
    return pl.pallas_call(
        functools.partial(kernel, dims, layer, has_back, has_front),
        out_shape=shapes,
        in_specs=specs,
        out_specs=[VMEM] * len(shapes),
        scratch_shapes=scratch,
        compiler_params=pltpu.CompilerParams(
            collective_id=number, has_side_effects=True, vmem_limit_bytes=40 * 2**20
        ),
    )(*operands)


def convolve(history, latest, weight):
    window = jnp.concatenate([history, latest[:, None, :]], axis=1)
    summed = jnp.sum(window.astype(jnp.float32) * weight.astype(jnp.float32)[None], axis=1)
    return (jax.nn.silu(summed), window[:, 1:])


def mixer(gate_in, conv_xv, conv_bv, conv_cv, step_raw, bias, log_rate, skip, gain, state_prev):
    seq_count = conv_xv.shape[0]
    heads_here = step_raw.shape[1]
    group_count = conv_bv.shape[1] // STATE
    per_group = heads_here // group_count
    step_size = jax.nn.softplus(step_raw + bias)
    decay_rate = jnp.exp(-step_size * jnp.exp(log_rate))
    x_heads = conv_xv.reshape(seq_count, group_count, per_group, HEAD_DIM)
    b_state = conv_bv.reshape(seq_count, group_count, 1, 1, STATE)
    c_state = conv_cv.reshape(seq_count, group_count, 1, 1, STATE)
    step_heads = step_size.reshape(seq_count, group_count, per_group, 1)
    decay_heads = decay_rate.reshape(seq_count, group_count, per_group, 1, 1)
    previous = state_prev.reshape(seq_count, group_count, per_group, HEAD_DIM, STATE)
    state_next = decay_heads * previous + (step_heads * x_heads)[..., None] * b_state
    readout = (
        jnp.sum(state_next * c_state, axis=-1)
        + skip.reshape(1, group_count, per_group, 1) * x_heads
    )
    gated_out = readout.reshape(seq_count, group_count, -1) * jax.nn.silu(
        gate_in.astype(jnp.float32)
    ).reshape(seq_count, group_count, -1)
    normed = gated_out * lax.rsqrt(
        jnp.mean(gated_out * gated_out, axis=-1, keepdims=True) + EPSILON
    )
    mixed_out = (normed.reshape(seq_count, -1) * gain.astype(jnp.float32)).astype(jnp.bfloat16)
    factors = (decay_heads[..., 0, 0], step_heads * x_heads, b_state[:, :, 0, 0, :])
    return mixed_out, factors


def body(
    tokens,
    norm_gain,
    w_z,
    w_x,
    w_b,
    w_c,
    w_dt,
    conv_x,
    conv_b,
    conv_c,
    dt_bias,
    a_log,
    d_skip,
    out_gain,
    w_out,
    ssm_state,
    state_x,
    state_b,
    state_c,
):
    tp, dp = lax.axis_size("tp"), lax.axis_size("dp")
    dims = (tp, dp, tokens.shape[1] * dp)
    weights = (w_z, w_x, w_b, w_c, jnp.swapaxes(w_dt, 1, 2))
    layers = w_z.shape[0]
    width, state_width = w_x.shape[2], w_b.shape[2]
    state_pad = padded(state_width)
    heads_here = dt_bias.shape[1]
    residual = tokens
    act, steps = exchange(dims, 0, 0, residual, None, None, norm_gain, weights)
    kept, factors = [], []
    for layer in range(layers):
        gate_in = act[:, 0:width]
        x_in = act[:, width : 2 * width]
        b_in = act[:, 2 * width : 2 * width + state_width]
        c_in = act[:, 2 * width + state_pad : 2 * width + state_pad + state_width]
        step_raw = lax.dynamic_slice_in_dim(steps, lax.axis_index("tp") * heads_here, heads_here, 1)
        conv_xv, kept_x = convolve(state_x[layer], x_in, conv_x[layer])
        conv_bv, kept_b = convolve(state_b[layer], b_in, conv_b[layer])
        conv_cv, kept_c = convolve(state_c[layer], c_in, conv_c[layer])
        mixed, pieces = mixer(
            gate_in,
            conv_xv,
            conv_bv,
            conv_cv,
            step_raw,
            dt_bias[layer],
            a_log[layer],
            d_skip[layer],
            out_gain[layer],
            ssm_state[layer],
        )
        kept.append((kept_x, kept_b, kept_c))
        factors.append(pieces)
        if layer + 1 < layers:
            residual, act, steps = exchange(
                dims, layer + 1, layer, residual, mixed, w_out, norm_gain, weights
            )
        else:
            (residual,) = exchange(dims, layer + 1, layer, residual, mixed, w_out, None, None)
    decay, added, inputs = (jnp.stack(each) for each in zip(*factors))
    decay, added, inputs = lax.optimization_barrier((decay, added, inputs))
    previous = ssm_state.reshape(decay.shape + (HEAD_DIM, STATE))
    state_next = decay[..., None, None] * previous + added[..., None] * inputs[:, :, :, None, None]
    saved = (jnp.stack(each) for each in zip(*kept))
    return (residual, state_next.reshape(ssm_state.shape), *saved)


def solution(mesh):
    placed = (
        P(("grp", "tp"), "dp"),
        P(None, "dp"),
        P(None, "dp", "tp"),
        P(None, "dp", "tp"),
        P(None, "dp", "tp"),
        P(None, "dp", "tp"),
        P(None, "dp", None),
        P(None, None, "tp"),
        P(None, None, "tp"),
        P(None, None, "tp"),
        P(None, "tp"),
        P(None, "tp"),
        P(None, "tp"),
        P(None, "tp"),
        P(None, "tp", "dp"),
        P(None, ("grp", "dp"), "tp", None, None),
        P(None, ("grp", "dp"), None, "tp"),
        P(None, ("grp", "dp"), None, "tp"),
        P(None, ("grp", "dp"), None, "tp"),
    )
    return jax.shard_map(
        body,
        mesh=mesh,
        in_specs=placed,
        out_specs=(
            P(("grp", "tp"), "dp"),
            P(None, ("grp", "dp"), "tp", None, None),
            P(None, ("grp", "dp"), None, "tp"),
            P(None, ("grp", "dp"), None, "tp"),
            P(None, ("grp", "dp"), None, "tp"),
        ),
        check_vma=False,
    )
```

time: 181 us -> 128 us (0.71)
  blocking collectives: 50.4 us -> 0 us
  waiting for transfers between devices: 50.2 us -> 0 us
  Pallas kernels: 0 us -> 41.4 us
  local copies, waits for them, and re-layouts: 9.09 us -> 29.7 us
  matrix products: 13.6 us -> 0 us
  between operations: 14.1 us -> 1.06 us
  other arithmetic: 42.1 us -> 54 us
    reduce_scatter x4 -> x0, waiting for transfers between devices: 50.2 us -> none  [the longest x2 25.5 us: body(): lax.psum_scatter(merged_terms, 'dp', scatter_dimension=0, tiled=True)]
    pallas_call x0 -> x3, Pallas kernels: none -> 41.4 us  [exchange(): pl.pallas_call(functools.partial(kernel, dims, layer, has_back, has_front...]
    all_gather x4 -> x0, blocking collectives: 39.1 us -> none  [the longest x2 28.3 us: body(): gathered_rows = lax.all_gather(residual, 'tp', axis=0, tiled=True)]
    dot_general x12 -> x0, matrix products: 13.6 us -> none  [the longest x10 11.7 us: body(): jnp.dot(rows_piece, matrix, preferred_element_type=jnp.float32)]
    add x0 -> x1, other arithmetic: none -> 13.1 us  [body(): decay[..., None, None] * previous]
    psum x2 -> x0, blocking collectives: 11.3 us -> none  [body(): everything = lax.psum(squares, 'dp')]
    unnamed x12 -> x45, local copies, waits for them, and re-layouts: 1.74 us -> 11.4 us
    another operation x9 -> x11, other arithmetic: 14.5 us -> 8.73 us  [the longest x8 7.18 us: body(): saved = (jnp.stack(each) for each in zip(*kept))]
  transfers between devices with their start and end apart: 4 -> 0, of which waited for: 4 -> 0; matrix products, arithmetic and copies ran while one was open for 12% -> 0% of each run, Pallas kernels for 0% -> 0%
where the time goes in v1:
time: 128 us; the launch traced here: 126 us
  other arithmetic  54 us (42%)
  Pallas kernels  41.4 us (32%)
  local copies, waits for them, and re-layouts  29.7 us (23%)
    pallas_call x3, Pallas kernels, exchange(): pl.pallas_call(functools.partial(kernel, dims, layer, has_back, has_front...  41.4 us
    reduce_sum x2, other arithmetic, mixer(): jnp.sum(state_next * c_state, axis=-1)  15.8 us
    add x1, other arithmetic, body(): decay[..., None, None] * previous  13.1 us
    unnamed x45, local copies, waits for them, and re-layouts  11.4 us
    another operation x8, other arithmetic, body(): saved = (jnp.stack(each) for each in zip(*kept))  7.18 us
    mul x3, other arithmetic, convolve(): window.astype(jnp.float32) * weight.astype(jnp.float32)[None]  3.9 us
    reduce_sum x5, other arithmetic, convolve(): jnp.sum(window.astype(jnp.float32) * weight.astype(jnp.float32)[None], ax...  3.14 us
    mul x4, other arithmetic, mixer(): step_heads * x_heads  2.92 us

profile of v1, /device:TPU:0, one launch (start us, length us, event | category | flops | bytes accessed | tf_op | source)
XLA Modules:
  0.0 126.2 jit_solution(1299729464078284435)
XLA Ops:
  1.6 1.3 %exponential_bitcast_fusion = (f32[16]{0:T(128)}, f32[16]{0:T(128)S(1)}, f32[16]{0:T(128)S(1)}, f32[16]{0:T(128)}) fusion(f32[2,16]{1,0:T(2,128)} %param.30, f32[2,16]{1,0:T(2,128)} %param.29), kind=kLoop, calls=%fused_computation.100 | loop fusion | bytes 512 | tf_op jit(solution)/shard_map/mul | solution.py:299
  5.2 1.3 %bitcast_convert_fusion.3 = (f32[4,256]{1,0:T(4,128)}, f32[4,256]{1,0:T(4,128)S(1)}) fusion(bf16[2,4,256]{2,1,0:T(4,128)(2,1)} %param.27), kind=kLoop, calls=%fused_computation.96 | loop fusion | flops 2048 | bytes 12288 | tf_op jit(solution)/shard_map/mul | solution.py:289
  6.5 1.3 %bitcast_convert_fusion.2 = (f32[4,256]{1,0:T(4,128)}, f32[4,256]{1,0:T(4,128)S(1)}) fusion(bf16[2,4,256]{2,1,0:T(4,128)(2,1)} %param.28), kind=kLoop, calls=%fused_computation.95 | loop fusion | flops 2048 | bytes 12288 | tf_op jit(solution)/shard_map/mul | solution.py:289
  7.7 1.4 %slice_convert_fusion = (f32[1,1024]{1,0:T(1,128)}, f32[1,1024]{1,0:T(1,128)}) fusion(bf16[2,1024]{1,0:T(2,128)(2,1)} %param.32), kind=kLoop, calls=%fused_computation.93 | loop fusion | flops 2048 | bytes 12288 | tf_op jit(solution)/shard_map/mul | solution.py:317
  9.1 1.3 %bitcast_convert_fusion = (f32[4,1024]{1,0:T(4,128)}, f32[4,1024]{1,0:T(4,128)}) fusion(bf16[2,4,1024]{2,1,0:T(4,128)(2,1)} %param.26), kind=kLoop, calls=%fused_computation.83 | loop fusion | flops 8192 | bytes 49152 | tf_op jit(solution)/shard_map/mul | solution.py:289
  10.4 1.4 %slice_bitcast_fusion.5 = (bf16[16,3,256]{2,0,1:T(8,128)(2,1)}, bf16[16,3,256]{2,0,1:T(8,128)(2,1)S(1)}) fusion(bf16[2,16,3,256]{3,1,2,0:T(8,128)(2,1)} %param.36), kind=kLoop, calls=%fused_computation.77 | loop fusion | bytes 98304 | tf_op jit(solution)/shard_map/squeeze | solution.py:360
  12.5 1.6 %copy-done = bf16[2,512,1024]{2,1,0:T(8,128)(2,1)S(1)} copy-done((bf16[2,512,1024]{2,1,0:T(8,128)(2,1)S(1)}, bf16[2,512,1024]{2,1,0:T(8,128)(2,1)}, u32[]{:S(2)}) %copy-start) | copy-done | bytes 2097176
  14.1 1.6 %copy-done.2 = bf16[2,512,1024]{2,1,0:T(8,128)(2,1)S(1)} copy-done((bf16[2,512,1024]{2,1,0:T(8,128)(2,1)S(1)}, bf16[2,512,1024]{2,1,0:T(8,128)(2,1)}, u32[]{:S(2)}) %copy-start.2) | copy-done | bytes 2097176
  15.7 1.0 copy-done.6
  16.8 1.0 copy-done.8
  17.8 0.9 copy-done.10
  20.1 13.6 %shard_map.218 = (bf16[16,2560]{1,0:T(8,128)(2,1)S(1)}, f32[16,128]{1,0:T(8,128)S(1)}) custom-call(bf16[16,512]{1,0:T(8,128)(2,1)S(1)} %copy-done.12, bf16[2,512]{1,0:T(2,128)(2,1)S(1)} %copy-done.14, bf16[2,512,1024]{2,1,0:T(8,128)(2,1)S(1)} %copy-done, bf16[2,512,1024]{2,1,0:T(8,128)(2,1)S(1)} %copy-done.2, bf16[2,512,256]{2,1,0:T(8,128)(2,1)S(1)} %copy-done.6, ...), custom_call_target="tpu_custom_call" | custom-call | tf_op jit(solution)/shard_map/pallas_call | solution.py:275
  38.2 1.4 %mul.512 = f32[16,4,4,64]{3,2,1,0:T(4,128)} broadcast(f32[16,4,64]{2,1,0:T(4,128)} %divide_multiply_fusion.9), dimensions={0,1,3} | broadcast | bytes 81920 | tf_op jit(solution)/shard_map/mul | solution.py:306
  39.7 1.4 %mul.521 = f32[16,4,4,64]{3,2,1,0:T(4,128)} broadcast(f32[16,4,64]{2,1,0:T(4,128)} %divide_multiply_fusion.8), dimensions={0,1,3} | broadcast | bytes 81920 | tf_op jit(solution)/shard_map/mul | solution.py:308
  41.1 1.6 %slice_bitcast_fusion = (bf16[16,3,1024]{2,0,1:T(8,128)(2,1)}, bf16[16,3,1024]{2,0,1:T(8,128)(2,1)S(1)}) fusion(bf16[2,16,3,1024]{3,1,2,0:T(8,128)(2,1)} %param.35), kind=kLoop, calls=%fused_computation.23 | loop fusion | bytes 393216 | tf_op jit(solution)/shard_map/squeeze | solution.py:359
  45.5 1.7 %fusion.1 = f32[1,16,4,4,64]{4,3,2,1,0:T(4,128)} fusion(f32[1,16,4,4,64]{4,3,2,1,0:T(4,128)} %reduce_sum.144, f32[16,4,4]{2,1,0:T(4,128)S(1)} %copy.27), kind=kLoop, calls=%fused_computation.16 | loop fusion | flops 81920 | bytes 132096 | tf_op jit(solution)/shard_map/mul | solution.py:306
  47.9 1.0 multiply_multiply_fusion.1
  48.9 8.3 %multiply_reduce_fusion.1 = f32[16,16,64]{2,1,0:T(8,128)} fusion(f32[2,16,16,64,64]{4,3,2,1,0:T(8,128)} %param.34, f32[16,16,64]{2,1,0:T(8,128)} %bitcast.85, f32[16,16,64]{2,1,0:T(8,128)} %bitcast.84, f32[16,16,64]{2,1,0:T(8,128)S(1)} %multiply_multiply_fusion.1, f32[16,16]{1,0:T(8,128)} %copy-done.17), kind=kLoop, calls=%fused_computation.2 | loop fusion | flops 5226496 | bytes 4457472 | tf_op jit(solution)/shard_map/reduce_sum | solution.py:308
  57.3 1.0 reduce_sum.130
  58.3 1.0 multiply_reduce_fusion.7
  59.3 1.0 reduce_sum.129
  61.2 1.6 %copy-done.3 = bf16[2,512,1024]{2,1,0:T(8,128)(2,1)S(1)} copy-done((bf16[2,512,1024]{2,1,0:T(8,128)(2,1)S(1)}, bf16[2,512,1024]{2,1,0:T(8,128)(2,1)}, u32[]{:S(2)}) %copy-start.3) | copy-done | bytes 2097176
  62.8 1.6 %copy-done.4 = bf16[2,1024,512]{2,1,0:T(8,128)(2,1)S(1)} copy-done((bf16[2,1024,512]{2,1,0:T(8,128)(2,1)S(1)}, bf16[2,1024,512]{2,1,0:T(8,128)(2,1)}, u32[]{:S(2)}) %copy-start.4) | copy-done | bytes 2097176
  64.4 19.2 %shard_map.219 = (bf16[16,512]{1,0:T(8,128)(2,1)S(1)}, bf16[16,2560]{1,0:T(8,128)(2,1)S(1)}, f32[16,128]{1,0:T(8,128)S(1)}) custom-call(bf16[16,512]{1,0:T(8,128)(2,1)S(1)} %copy-done.13, bf16[16,1024]{1,0:T(8,128)(2,1)S(1)} %multiply_convert_fusion.1.refs_1_, bf16[2,1024,512]{2,1,0:T(8,128)(2,1)S(1)} %copy-done.4, bf16[2,512]{1,0:T(2,128)(2,1)S(1)} %copy-done.15, ...), custom_call_target="tpu_custom_call" | custom-call | tf_op jit(solution)/shard_map/pallas_call | solution.py:275
  83.7 0.9 multiply_exponential_fusion
  86.9 1.4 %pad_maximum_fusion.5 = bf16[2,16,3,256]{3,1,2,0:T(8,128)(2,1)} fusion(bf16[1,16,3,256]{3,1,2,0:T(8,128)(2,1)S(1)} %fusion.15, bf16[1,16,3,256]{3,1,2,0:T(8,128)(2,1)} %get-tuple-element.52), kind=kLoop, calls=%fused_computation.46 | loop fusion | flops 24576 | bytes 98304 | tf_op jit(solution)/shard_map/stack | solution.py:386
  89.0 1.4 %pad_maximum_fusion.6 = bf16[2,16,3,256]{3,1,2,0:T(8,128)(2,1)} fusion(bf16[1,16,3,256]{3,1,2,0:T(8,128)(2,1)S(1)} %fusion.13, bf16[1,16,3,256]{3,1,2,0:T(8,128)(2,1)} %get-tuple-element.51), kind=kLoop, calls=%fused_computation.47 | loop fusion | flops 24576 | bytes 98304 | tf_op jit(solution)/shard_map/stack | solution.py:386
  91.6 0.9 multiply_reduce_fusion.2
  93.4 1.6 %pad_maximum_fusion.1 = bf16[2,16,3,1024]{3,1,2,0:T(8,128)(2,1)} fusion(bf16[1,16,3,1024]{3,1,2,0:T(8,128)(2,1)S(1)} %fusion.3, bf16[1,16,3,1024]{3,1,2,0:T(8,128)(2,1)} %fusion.5), kind=kLoop, calls=%fused_computation.6 | loop fusion | flops 98304 | bytes 393216 | tf_op jit(solution)/shard_map/stack | solution.py:386
  95.8 7.5 %multiply_reduce_fusion = f32[16,16,64]{2,1,0:T(8,128)S(1)} fusion(f32[2,16,16,64,64]{4,3,2,1,0:T(8,128)} %param.34, f32[16,16,64]{2,1,0:T(8,128)S(1)} %bitcast.87, f32[16,16,64]{2,1,0:T(8,128)S(1)} %bitcast.86, f32[16,16,64]{2,1,0:T(8,128)S(1)} %multiply_multiply_fusion, f32[16,16]{1,0:T(8,128)S(1)} %get-tuple-element.23), kind=kLoop, calls=%fused_computation.1 | loop fusion | flops 5226496 | bytes 4457472 | tf_op jit(solution)/shard_map/reduce_sum | solution.py:308
  103.8 8.6 %shard_map.220 = bf16[16,512]{1,0:T(8,128)(2,1)S(1)} custom-call(bf16[16,512]{1,0:T(8,128)(2,1)S(1)} %get-tuple-element.15.refs_0_, bf16[16,1024]{1,0:T(8,128)(2,1)S(1)} %multiply_convert_fusion.refs_1_, bf16[2,1024,512]{2,1,0:T(8,128)(2,1)S(1)} %copy-done.5), custom_call_target="tpu_custom_call" | custom-call | tf_op jit(solution)/shard_map/pallas_call | solution.py:275
  112.5 13.1 %multiply_add_fusion = f32[2,16,16,64,64]{4,3,2,1,0:T(8,128)} fusion(f32[2,16,16,64,64]{4,3,2,1,0:T(8,128)} %param.34, f32[2,16,16,64]{3,2,1,0:T(8,128)S(1)} %bitcast.82, f32[2,16,16,64]{3,2,1,0:T(8,128)S(1)} %bitcast.83, f32[2,16,16]{2,1,0:T(8,128)S(1)} %copy.30), kind=kLoop, calls=%fused_computation | loop fusion | flops 6291456 | bytes 17041408 | tf_op jit(solution)/shard_map/add | solution.py:385
  (108 shorter events, 21.2 us)
Async XLA Ops:
  12.5 1.6 %copy-start = (bf16[2,512,1024]{2,1,0:T(8,128)(2,1)S(1)}, bf16[2,512,1024]{2,1,0:T(8,128)(2,1)}, u32[]{:S(2)}) copy-start(bf16[2,512,1024]{2,1,0:T(8,128)(2,1)} %refs_4_.3) | copy-start | bytes 6291460
  14.1 1.6 %copy-start.2 = (bf16[2,512,1024]{2,1,0:T(8,128)(2,1)S(1)}, bf16[2,512,1024]{2,1,0:T(8,128)(2,1)}, u32[]{:S(2)}) copy-start(bf16[2,512,1024]{2,1,0:T(8,128)(2,1)} %refs_5_.3) | copy-start | bytes 6291460
  15.7 1.0 copy-start.6
  16.8 1.0 copy-start.8
  17.8 0.9 copy-start.10
  18.7 0.7 copy-start.12
  19.4 0.7 copy-start.14
  20.1 41.1 %copy-start.1 = (bf16[2,512,1024]{2,1,0:T(8,128)(2,1)S(1)}, bf16[2,512,1024]{2,1,0:T(8,128)(2,1)}, u32[]{:S(2)}) copy-start(bf16[2,512,1024]{2,1,0:T(8,128)(2,1)} %refs_4_.3) | copy-start | bytes 6291460
  20.1 41.1 %copy-start.7 = (bf16[2,512,256]{2,1,0:T(8,128)(2,1)S(1)}, bf16[2,512,256]{2,1,0:T(8,128)(2,1)}, u32[]{:S(2)}) copy-start(bf16[2,512,256]{2,1,0:T(8,128)(2,1)} %refs_6_.1) | copy-start | bytes 1572868
  20.1 41.1 %copy-start.9 = (bf16[2,512,256]{2,1,0:T(8,128)(2,1)S(1)}, bf16[2,512,256]{2,1,0:T(8,128)(2,1)}, u32[]{:S(2)}) copy-start(bf16[2,512,256]{2,1,0:T(8,128)(2,1)} %refs_7_.1) | copy-start | bytes 1572868
  20.1 41.1 %copy-start.11 = (bf16[2,512,64]{1,2,0:T(8,128)(2,1)S(1)}, bf16[2,512,64]{1,2,0:T(8,128)(2,1)}, u32[]{:S(2)}) copy-start(bf16[2,512,64]{1,2,0:T(8,128)(2,1)} %param.25) | copy-start | bytes 393220
  20.1 41.1 %copy-start.13 = (bf16[16,512]{1,0:T(8,128)(2,1)S(1)}, bf16[16,512]{1,0:T(8,128)(2,1)}, u32[]{:S(2)}) copy-start(bf16[16,512]{1,0:T(8,128)(2,1)} %refs_0_.3) | copy-start | bytes 49156
  20.1 41.1 %copy-start.15 = (bf16[2,512]{1,0:T(2,128)(2,1)S(1)}, bf16[2,512]{1,0:T(2,128)(2,1)}, u32[]{:S(2)}) copy-start(bf16[2,512]{1,0:T(2,128)(2,1)} %refs_3_.3) | copy-start | bytes 6148
  33.8 0.8 copy-start.17
  33.8 0.8 copy-start.18
  61.2 1.6 %copy-start.3 = (bf16[2,512,1024]{2,1,0:T(8,128)(2,1)S(1)}, bf16[2,512,1024]{2,1,0:T(8,128)(2,1)}, u32[]{:S(2)}) copy-start(bf16[2,512,1024]{2,1,0:T(8,128)(2,1)} %refs_5_.3) | copy-start | bytes 6291460
  62.8 1.6 %copy-start.4 = (bf16[2,1024,512]{2,1,0:T(8,128)(2,1)S(1)}, bf16[2,1024,512]{2,1,0:T(8,128)(2,1)}, u32[]{:S(2)}) copy-start(bf16[2,1024,512]{2,1,0:T(8,128)(2,1)} %refs_2_.5) | copy-start | bytes 6291460
  64.4 31.0 %copy-start.16 = (f32[1,16,4,4,64]{4,3,2,1,0:T(4,128)S(1)}, f32[1,16,4,4,64]{4,3,2,1,0:T(4,128)}, u32[]{:S(2)}) copy-start(f32[1,16,4,4,64]{4,3,2,1,0:T(4,128)} %fusion.1) | copy-start | bytes 196612
  83.6 19.7 %copy-start.20 = (f32[4,256]{1,0:T(4,128)S(1)}, f32[4,256]{1,0:T(4,128)}, u32[]{:S(2)}) copy-start(f32[4,256]{1,0:T(4,128)} %mul.585) | copy-start | bytes 12292
  83.7 20.1 %copy-start.19 = (f32[1,1024]{1,0:T(1,128)S(1)}, f32[1,1024]{1,0:T(1,128)}, u32[]{:S(2)}) copy-start(f32[1,1024]{1,0:T(1,128)} %get-tuple-element.39) | copy-start | bytes 12292
  83.7 20.1 %copy-start.5 = (bf16[2,1024,512]{2,1,0:T(8,128)(2,1)S(1)}, bf16[2,1024,512]{2,1,0:T(8,128)(2,1)}, u32[]{:S(2)}) copy-start(bf16[2,1024,512]{2,1,0:T(8,128)(2,1)} %refs_2_.5) | copy-start | bytes 6291460

commit v2 on v1

--- a/solution.py
+++ b/solution.py
@@ -12,7 +12,7 @@
 LANES = 128
 EPSILON = 1e-05
 MESH = pl.DeviceIdType.MESH
-HBM = pl.BlockSpec(memory_space=pl.ANY)
+HBM = pl.BlockSpec(memory_space=pltpu.HBM)
 VMEM = pl.BlockSpec(memory_space=pltpu.VMEM)
 
 
@@ -120,7 +120,8 @@
     for k in range(1, dp):
         side_sum = side_sum + side_got[k - 1]
     row_scale = lax.rsqrt(side_sum[:, LANES : LANES + 1] / features + EPSILON)
-    step_ref[...] = side_sum[:, 0:LANES] * row_scale
+    shift = lax.rem(LANES - me_tp * (dt_width // tp), LANES)
+    step_ref[...] = pltpu.roll(side_sum[:, 0:LANES] * row_scale, shift, 1)
     edges = (0, width, total.shape[2])
     for piece in range(2):
         for copy in copies[(piece + 1) * (dp - 1) : (piece + 2) * (dp - 1)]:
@@ -279,44 +280,126 @@
         out_specs=[VMEM] * len(shapes),
         scratch_shapes=scratch,
         compiler_params=pltpu.CompilerParams(
-            collective_id=number, has_side_effects=True, vmem_limit_bytes=40 * 2**20
+            collective_id=number, has_side_effects=True, vmem_limit_bytes=56 * 2**20
         ),
     )(*operands)
 
 
-def convolve(history, latest, weight):
-    window = jnp.concatenate([history, latest[:, None, :]], axis=1)
-    summed = jnp.sum(window.astype(jnp.float32) * weight.astype(jnp.float32)[None], axis=1)
-    return (jax.nn.silu(summed), window[:, 1:])
-
-
-def mixer(gate_in, conv_xv, conv_bv, conv_cv, step_raw, bias, log_rate, skip, gain, state_prev):
-    seq_count = conv_xv.shape[0]
-    heads_here = step_raw.shape[1]
-    group_count = conv_bv.shape[1] // STATE
-    per_group = heads_here // group_count
-    step_size = jax.nn.softplus(step_raw + bias)
-    decay_rate = jnp.exp(-step_size * jnp.exp(log_rate))
-    x_heads = conv_xv.reshape(seq_count, group_count, per_group, HEAD_DIM)
-    b_state = conv_bv.reshape(seq_count, group_count, 1, 1, STATE)
-    c_state = conv_cv.reshape(seq_count, group_count, 1, 1, STATE)
-    step_heads = step_size.reshape(seq_count, group_count, per_group, 1)
-    decay_heads = decay_rate.reshape(seq_count, group_count, per_group, 1, 1)
-    previous = state_prev.reshape(seq_count, group_count, per_group, HEAD_DIM, STATE)
-    state_next = decay_heads * previous + (step_heads * x_heads)[..., None] * b_state
-    readout = (
-        jnp.sum(state_next * c_state, axis=-1)
-        + skip.reshape(1, group_count, per_group, 1) * x_heads
+def convolve(history_ref, latest, taps_ref, layer, kept_ref):
+    weight = taps_ref[layer].astype(jnp.float32)
+    old = history_ref.shape[1]
+    summed = latest.astype(jnp.float32) * weight[old : old + 1]
+    for k in range(old):
+        summed = summed + history_ref[0, k].astype(jnp.float32) * weight[k : k + 1]
+    for k in range(1, old):
+        kept_ref[0, k - 1] = history_ref[0, k]
+    kept_ref[0, old - 1] = latest
+    return summed * jax.nn.sigmoid(summed)
+
+
+def mix_kernel(layer, heads_step, aliased, *refs):
+    act, steps, tap_x, tap_b, tap_c, bias, rate, skip, gain, prev, old_x, old_b, old_c = refs[:13]
+    mixed, state, kept_x, kept_b, kept_c = refs[13 + aliased : 18 + aliased]
+    skipped, factors, b_rows, c_rows, read = refs[18 + aliased :]
+    seqs, width = mixed.shape
+    heads = bias.shape[1]
+    groups = b_rows.shape[0]
+    per_group = heads // groups
+    state_width = kept_b.shape[3]
+    at = pl.program_id(0)
+
+    @pl.when(at == 0)
+    def _():
+        raw = steps[:, 0:heads] + bias[layer : layer + 1, :]
+        size = jnp.maximum(raw, 0.0) + jnp.log1p(jnp.exp(-jnp.abs(raw)))
+        decay = jnp.exp(-size * jnp.exp(rate[layer : layer + 1, :]))
+        skips = jnp.broadcast_to(skip[layer : layer + 1, :], (8, heads))
+        stacked = jnp.concatenate([size, decay, skips], axis=0)
+        row = lax.broadcasted_iota(jnp.int32, (heads, width), 0)
+        lane = lax.broadcasted_iota(jnp.int32, (heads, width), 1)
+        first = row * HEAD_DIM
+        spread = jnp.where((lane >= first) & (lane < first + HEAD_DIM), 1.0, 0.0)
+        wide = jnp.dot(
+            stacked, spread, precision=lax.Precision.HIGHEST, preferred_element_type=jnp.float32
+        )
+        conv = convolve(old_x, act[:, width : 2 * width], tap_x, layer, kept_x)
+        skipped[...] = wide[2 * seqs : 2 * seqs + 1] * conv
+        both = jnp.concatenate([wide[0:seqs] * conv, wide[seqs : 2 * seqs]], axis=0)
+        factors[...] = both.T
+        begin = 2 * width
+        for target, old, tap, kept in ((b_rows, old_b, tap_b, kept_b), (c_rows, old_c, tap_c, kept_c)):
+            conv = convolve(old, act[:, begin : begin + state_width], tap, layer, kept)
+            for g in range(groups):
+                target[g] = conv[:, g * STATE : (g + 1) * STATE]
+            begin += padded(state_width)
+
+    group = at * heads_step // per_group
+    b_here, c_here = b_rows[group], c_rows[group]
+    spot = lax.broadcasted_iota(jnp.int32, (HEAD_DIM, seqs), 1)
+    for j in range(heads_step):
+        first = pl.multiple_of((at * heads_step + j) * HEAD_DIM, HEAD_DIM)
+        columns = factors[pl.ds(first, HEAD_DIM), :]
+        taken = jnp.zeros((HEAD_DIM, seqs), jnp.float32)
+        for s in range(seqs):
+            fade = columns[:, seqs + s : seqs + s + 1]
+            new = fade * prev[0, s, j] + columns[:, s : s + 1] * b_here[s : s + 1, :]
+            state[0, s, j] = new
+            summed = jnp.sum(new * c_here[s : s + 1, :], axis=1, keepdims=True)
+            taken = jnp.where(spot == s, summed, taken)
+        read[pl.ds(first, HEAD_DIM), :] = taken
+
+    @pl.when(at == pl.num_programs(0) - 1)
+    def _():
+        gate = act[:, 0:width].astype(jnp.float32)
+        gated = (read[...].T + skipped[...]) * (gate * jax.nn.sigmoid(gate))
+        span = per_group * HEAD_DIM
+        for g in range(groups):
+            part = gated[:, g * span : (g + 1) * span]
+            scale = lax.rsqrt(jnp.mean(part * part, axis=1, keepdims=True) + EPSILON)
+            gains = gain[layer : layer + 1, g * span : (g + 1) * span].astype(jnp.float32)
+            mixed[:, g * span : (g + 1) * span] = (part * scale * gains).astype(jnp.bfloat16)
+
+
+def mix(layer, act, steps, params, state, olds, carried):
+    seqs, heads = state.shape[1:3]
+    width, state_width = olds[0].shape[3], olds[1].shape[3]
+    groups = state_width // STATE
+    per_group = heads // groups
+    heads_step = 2 if per_group % 2 == 0 else 1
+    seqs_dim = lambda ref: (1,) + ref.shape[1:]
+    whole = lambda ref: pl.BlockSpec(ref.shape, lambda i, n=ref.ndim: (0,) * n)
+    at_layer = lambda ref: pl.BlockSpec(seqs_dim(ref), lambda i, n=ref.ndim: (layer,) + (0,) * (n - 1))
+    tile = pl.BlockSpec(
+        (1, seqs, heads_step, HEAD_DIM, STATE), lambda i: (layer, 0, i, 0, 0)
     )
-    gated_out = readout.reshape(seq_count, group_count, -1) * jax.nn.silu(
-        gate_in.astype(jnp.float32)
-    ).reshape(seq_count, group_count, -1)
-    normed = gated_out * lax.rsqrt(
-        jnp.mean(gated_out * gated_out, axis=-1, keepdims=True) + EPSILON
-    )
-    mixed_out = (normed.reshape(seq_count, -1) * gain.astype(jnp.float32)).astype(jnp.bfloat16)
-    factors = (decay_heads[..., 0, 0], step_heads * x_heads, b_state[:, :, 0, 0, :])
-    return mixed_out, factors
+    operands = [act, steps, *params, state, *olds]
+    specs = [whole(x) for x in (act, steps, *params)] + [tile] + [at_layer(x) for x in olds]
+    aliases = {}
+    if carried is not None:
+        aliases = {len(operands) + i: 1 + i for i in range(4)}
+        operands += carried
+        specs += [pl.BlockSpec(memory_space=pl.ANY)] * 4
+    kinds = [jax.ShapeDtypeStruct(x.shape, x.dtype) for x in (state, *olds)]
+    mixed = jax.ShapeDtypeStruct((seqs, width), jnp.bfloat16)
+    f32 = jnp.float32
+    return pl.pallas_call(
+        functools.partial(mix_kernel, layer, heads_step, len(aliases)),
+        grid=(heads // heads_step,),
+        out_shape=[mixed] + kinds,
+        in_specs=specs,
+        out_specs=[whole(mixed), tile] + [at_layer(x) for x in olds],
+        scratch_shapes=[
+            pltpu.VMEM((seqs, width), f32),
+            pltpu.VMEM((width, 2 * seqs), f32),
+            pltpu.VMEM((groups, seqs, STATE), f32),
+            pltpu.VMEM((groups, seqs, STATE), f32),
+            pltpu.VMEM((width, seqs), f32),
+        ],
+        input_output_aliases=aliases,
+        compiler_params=pltpu.CompilerParams(
+            dimension_semantics=("arbitrary",), vmem_limit_bytes=56 * 2**20
+        ),
+    )(*operands)
 
 
 def body(
@@ -344,47 +427,20 @@
     dims = (tp, dp, tokens.shape[1] * dp)
     weights = (w_z, w_x, w_b, w_c, jnp.swapaxes(w_dt, 1, 2))
     layers = w_z.shape[0]
-    width, state_width = w_x.shape[2], w_b.shape[2]
-    state_pad = padded(state_width)
-    heads_here = dt_bias.shape[1]
+    params = (conv_x, conv_b, conv_c, dt_bias, a_log, d_skip, out_gain)
+    olds = [jnp.swapaxes(x, 1, 2) for x in (state_x, state_b, state_c)]
     residual = tokens
     act, steps = exchange(dims, 0, 0, residual, None, None, norm_gain, weights)
-    kept, factors = [], []
+    carried = None
     for layer in range(layers):
-        gate_in = act[:, 0:width]
-        x_in = act[:, width : 2 * width]
-        b_in = act[:, 2 * width : 2 * width + state_width]
-        c_in = act[:, 2 * width + state_pad : 2 * width + state_pad + state_width]
-        step_raw = lax.dynamic_slice_in_dim(steps, lax.axis_index("tp") * heads_here, heads_here, 1)
-        conv_xv, kept_x = convolve(state_x[layer], x_in, conv_x[layer])
-        conv_bv, kept_b = convolve(state_b[layer], b_in, conv_b[layer])
-        conv_cv, kept_c = convolve(state_c[layer], c_in, conv_c[layer])
-        mixed, pieces = mixer(
-            gate_in,
-            conv_xv,
-            conv_bv,
-            conv_cv,
-            step_raw,
-            dt_bias[layer],
-            a_log[layer],
-            d_skip[layer],
-            out_gain[layer],
-            ssm_state[layer],
-        )
-        kept.append((kept_x, kept_b, kept_c))
-        factors.append(pieces)
+        mixed, *carried = mix(layer, act, steps, params, ssm_state, olds, carried)
         if layer + 1 < layers:
             residual, act, steps = exchange(
                 dims, layer + 1, layer, residual, mixed, w_out, norm_gain, weights
             )
         else:
             (residual,) = exchange(dims, layer + 1, layer, residual, mixed, w_out, None, None)
-    decay, added, inputs = (jnp.stack(each) for each in zip(*factors))
-    decay, added, inputs = lax.optimization_barrier((decay, added, inputs))
-    previous = ssm_state.reshape(decay.shape + (HEAD_DIM, STATE))
-    state_next = decay[..., None, None] * previous + added[..., None] * inputs[:, :, :, None, None]
-    saved = (jnp.stack(each) for each in zip(*kept))
-    return (residual, state_next.reshape(ssm_state.shape), *saved)
+    return (residual, carried[0], *(jnp.swapaxes(x, 1, 2) for x in carried[1:]))
 
 
 def solution(mesh):

time: 128 us -> 103 us (0.80); the launches traced: 126 us -> 103 us
  Pallas kernels: 41.4 us -> 101 us
  other arithmetic: 54 us -> 0 us
  local copies, waits for them, and re-layouts: 29.7 us -> 1.32 us
    pallas_call x0 -> x2, Pallas kernels: none -> 55.8 us  [mix(): pl.pallas_call(functools.partial(mix_kernel, layer, heads_step, len(alias...]
    reduce_sum x9 -> x0, other arithmetic: 20.1 us -> none  [the longest x2 15.8 us: mixer(): jnp.sum(state_next * c_state, axis=-1)]
    add x1 -> x0, other arithmetic: 13.1 us -> none  [body(): decay[..., None, None] * previous]
    mul x16 -> x0, other arithmetic: 10.3 us -> none  [the longest x3 3.9 us: convolve(): window.astype(jnp.float32) * weight.astype(jnp.float32)[None]]
    unnamed x45 -> x1, local copies, waits for them, and re-layouts: 11.4 us -> 1.32 us
    another operation x11 -> x0, other arithmetic: 8.73 us -> none  [the longest x8 7.18 us: body(): saved = (jnp.stack(each) for each in zip(*kept))]
    mul x19 -> x0, local copies, waits for them, and re-layouts: 7.16 us -> none  [the longest x8 2.4 us: mixer(): skip.reshape(1, group_count, per_group, 1) * x_heads]
    reduce_sum x16 -> x0, local copies, waits for them, and re-layouts: 5.07 us -> none  [the longest x12 2.87 us: convolve(): jnp.sum(window.astype(jnp.float32) * weight.astype(jnp.float32)[None], ax...]
where the time goes in v2:
time: 103 us
  Pallas kernels  101 us (98%)
  local copies, waits for them, and re-layouts  1.32 us (1%)
    pallas_call x2, Pallas kernels, mix(): pl.pallas_call(functools.partial(mix_kernel, layer, heads_step, len(alias...  55.8 us
    pallas_call x3, Pallas kernels, exchange(): pl.pallas_call(functools.partial(kernel, dims, layer, has_back, has_front...  44.8 us

profile of v2, /device:TPU:0, one launch (start us, length us, event | category | flops | bytes accessed | tf_op | source)
XLA Modules:
  0.0 102.6 jit_solution(8621347073377885384)
XLA Ops:
  0.6 14.6 %shard_map.218 = (bf16[16,2560]{1,0:T(8,128)(2,1)}, f32[16,128]{1,0:T(8,128)}) custom-call(bf16[16,512]{1,0:T(8,128)(2,1)} %refs_0_.3, bf16[2,512]{1,0:T(2,128)(2,1)} %refs_3_.6, bf16[2,512,1024]{2,1,0:T(8,128)(2,1)} %refs_4_.6, bf16[2,512,1024]{2,1,0:T(8,128)(2,1)} %refs_5_.6, bf16[2,512,256]{2,1,0:T(8,128)(2,1)} %refs_6_.4, bf16[2,512,256]{2,1,0:T(8,128)(2,1)} %refs_7_.4, ...), custom_call_target="tpu_custom_call" | custom-call | tf_op jit(solution)/shard_map/pallas_call | solution.py:276
  15.2 27.9 %shard_map.219 = (bf16[16,1024]{1,0:T(8,128)(2,1)}, f32[2,16,16,64,64]{4,3,2,1,0:T(8,128)}, bf16[2,3,16,1024]{3,2,1,0:T(8,128)(2,1)}, bf16[2,3,16,256]{3,2,1,0:T(8,128)(2,1)}, bf16[2,3,16,256]{3,2,1,0:T(8,128)(2,1)}) custom-call(bf16[16,2560]{1,0:T(8,128)(2,1)} %get-tuple-element.20.refs_0_, f32[16,128]{1,0:T(8,128)} %get-tuple-element.21.refs_1_, ...), custom_call_target="tpu_custom_call" | custom-call | tf_op jit(solution)/shard_map/pallas_call | solution.py:385
  43.2 20.3 %shard_map.220 = (bf16[16,512]{1,0:T(8,128)(2,1)}, bf16[16,2560]{1,0:T(8,128)(2,1)}, f32[16,128]{1,0:T(8,128)}) custom-call(bf16[16,512]{1,0:T(8,128)(2,1)} %refs_0_.3, bf16[16,1024]{1,0:T(8,128)(2,1)} %get-tuple-element.22.refs_1_, bf16[2,1024,512]{2,1,0:T(8,128)(2,1)} %refs_2_.9, bf16[2,512]{1,0:T(2,128)(2,1)} %refs_3_.6, bf16[2,512,1024]{2,1,0:T(8,128)(2,1)} %refs_4_.6, ...), custom_call_target="tpu_custom_call" | custom-call | tf_op jit(solution)/shard_map/pallas_call | solution.py:276
  63.5 27.9 %shard_map.221 = (bf16[16,1024]{1,0:T(8,128)(2,1)}, f32[2,16,16,64,64]{4,3,2,1,0:T(8,128)}, bf16[2,3,16,1024]{3,2,1,0:T(8,128)(2,1)}, bf16[2,3,16,256]{3,2,1,0:T(8,128)(2,1)}, bf16[2,3,16,256]{3,2,1,0:T(8,128)(2,1)}) custom-call(bf16[16,2560]{1,0:T(8,128)(2,1)} %get-tuple-element.24.refs_, ...), custom_call_target="tpu_custom_call", output_to_operand_aliasing={{1}: (13, {}), {2}: (14, {}), {3}: (15, {}), {4}: (16, {})} | custom-call | tf_op jit(solution)/shard_map/pallas_call | solution.py:385
  91.4 9.9 %shard_map.222 = bf16[16,512]{1,0:T(8,128)(2,1)} custom-call(bf16[16,512]{1,0:T(8,128)(2,1)} %get-tuple-element.23.refs_0_, bf16[16,1024]{1,0:T(8,128)(2,1)} %get-tuple-element.30.refs_1_, bf16[2,1024,512]{2,1,0:T(8,128)(2,1)} %refs_2_.9), custom_call_target="tpu_custom_call" | custom-call | tf_op jit(solution)/shard_map/pallas_call | solution.py:276
  101.3 1.3 %copy.33 = bf16[16,512]{1,0:T(8,128)(2,1)} copy(bf16[16,512]{1,0:T(8,128)(2,1)} %shard_map.222) | data formatting | bytes 32768

commit v3 on v2

--- a/solution.py
+++ b/solution.py
@@ -334,17 +334,22 @@
             begin += padded(state_width)
 
     group = at * heads_step // per_group
-    b_here, c_here = b_rows[group], c_rows[group]
+    b_here, c_half = b_rows[group], c_rows[group].astype(jnp.bfloat16)
     spot = lax.broadcasted_iota(jnp.int32, (HEAD_DIM, seqs), 1)
     for j in range(heads_step):
         first = pl.multiple_of((at * heads_step + j) * HEAD_DIM, HEAD_DIM)
         columns = factors[pl.ds(first, HEAD_DIM), :]
         taken = jnp.zeros((HEAD_DIM, seqs), jnp.float32)
         for s in range(seqs):
-            fade = columns[:, seqs + s : seqs + s + 1]
+            fade = columns[0:1, seqs + s : seqs + s + 1]
             new = fade * prev[0, s, j] + columns[:, s : s + 1] * b_here[s : s + 1, :]
             state[0, s, j] = new
-            summed = jnp.sum(new * c_here[s : s + 1, :], axis=1, keepdims=True)
+            summed = lax.dot_general(
+                new.astype(jnp.bfloat16),
+                c_half,
+                (((1,), (1,)), ((), ())),
+                preferred_element_type=jnp.float32,
+            )
             taken = jnp.where(spot == s, summed, taken)
         read[pl.ds(first, HEAD_DIM), :] = taken
 

time: 103 us -> 70.3 us (0.68)
  Pallas kernels: 101 us -> 67.6 us
    pallas_call x2, Pallas kernels: 55.8 us -> 22.8 us  [mix(): pl.pallas_call(functools.partial(mix_kernel, layer, heads_step, len(alias...]
where the time goes in v3:
time: 70.3 us; the launch traced here: 69.6 us
  Pallas kernels  67.6 us (96%)
  local copies, waits for them, and re-layouts  1.32 us (2%)
    pallas_call x3, Pallas kernels, exchange(): pl.pallas_call(functools.partial(kernel, dims, layer, has_back, has_front...  44.8 us
    pallas_call x2, Pallas kernels, mix(): pl.pallas_call(functools.partial(mix_kernel, layer, heads_step, len(alias...  22.8 us

profile of v3, /device:TPU:0, one launch (start us, length us, event | category | flops | bytes accessed | tf_op | source)
XLA Modules:
  0.0 69.6 jit_solution(7879121538913196173)
XLA Ops:
  0.6 14.6 %shard_map.218 = (bf16[16,2560]{1,0:T(8,128)(2,1)}, f32[16,128]{1,0:T(8,128)}) custom-call(bf16[16,512]{1,0:T(8,128)(2,1)} %refs_0_.3, bf16[2,512]{1,0:T(2,128)(2,1)} %refs_3_.6, bf16[2,512,1024]{2,1,0:T(8,128)(2,1)} %refs_4_.6, bf16[2,512,1024]{2,1,0:T(8,128)(2,1)} %refs_5_.6, bf16[2,512,256]{2,1,0:T(8,128)(2,1)} %refs_6_.4, bf16[2,512,256]{2,1,0:T(8,128)(2,1)} %refs_7_.4, ...), custom_call_target="tpu_custom_call" | custom-call | tf_op jit(solution)/shard_map/pallas_call | solution.py:276
  15.2 11.4 %shard_map.219 = (bf16[16,1024]{1,0:T(8,128)(2,1)}, f32[2,16,16,64,64]{4,3,2,1,0:T(8,128)}, bf16[2,3,16,1024]{3,2,1,0:T(8,128)(2,1)}, bf16[2,3,16,256]{3,2,1,0:T(8,128)(2,1)}, bf16[2,3,16,256]{3,2,1,0:T(8,128)(2,1)}) custom-call(bf16[16,2560]{1,0:T(8,128)(2,1)} %get-tuple-element.20.refs_0_, f32[16,128]{1,0:T(8,128)} %get-tuple-element.21.refs_1_, ...), custom_call_target="tpu_custom_call" | custom-call | tf_op jit(solution)/shard_map/pallas_call | solution.py:390
  26.6 20.3 %shard_map.220 = (bf16[16,512]{1,0:T(8,128)(2,1)}, bf16[16,2560]{1,0:T(8,128)(2,1)}, f32[16,128]{1,0:T(8,128)}) custom-call(bf16[16,512]{1,0:T(8,128)(2,1)} %refs_0_.3, bf16[16,1024]{1,0:T(8,128)(2,1)} %get-tuple-element.22.refs_1_, bf16[2,1024,512]{2,1,0:T(8,128)(2,1)} %refs_2_.9, bf16[2,512]{1,0:T(2,128)(2,1)} %refs_3_.6, bf16[2,512,1024]{2,1,0:T(8,128)(2,1)} %refs_4_.6, ...), custom_call_target="tpu_custom_call" | custom-call | tf_op jit(solution)/shard_map/pallas_call | solution.py:276
  47.0 11.4 %shard_map.221 = (bf16[16,1024]{1,0:T(8,128)(2,1)}, f32[2,16,16,64,64]{4,3,2,1,0:T(8,128)}, bf16[2,3,16,1024]{3,2,1,0:T(8,128)(2,1)}, bf16[2,3,16,256]{3,2,1,0:T(8,128)(2,1)}, bf16[2,3,16,256]{3,2,1,0:T(8,128)(2,1)}) custom-call(bf16[16,2560]{1,0:T(8,128)(2,1)} %get-tuple-element.24.refs_, ...), custom_call_target="tpu_custom_call", output_to_operand_aliasing={{1}: (13, {}), {2}: (14, {}), {3}: (15, {}), {4}: (16, {})} | custom-call | tf_op jit(solution)/shard_map/pallas_call | solution.py:390
  58.3 9.9 %shard_map.222 = bf16[16,512]{1,0:T(8,128)(2,1)} custom-call(bf16[16,512]{1,0:T(8,128)(2,1)} %get-tuple-element.23.refs_0_, bf16[16,1024]{1,0:T(8,128)(2,1)} %get-tuple-element.30.refs_1_, bf16[2,1024,512]{2,1,0:T(8,128)(2,1)} %refs_2_.9), custom_call_target="tpu_custom_call" | custom-call | tf_op jit(solution)/shard_map/pallas_call | solution.py:276
  68.2 1.3 %copy.33 = bf16[16,512]{1,0:T(8,128)(2,1)} copy(bf16[16,512]{1,0:T(8,128)(2,1)} %shard_map.222) | data formatting | bytes 32768
